TPU v7x, 32 devices: a whole 2x2x4 slice. The times are simulated.
32 devices in a mesh: rep: 2 (over x), fs: 8 (over z, y), tp: 2 (over core).
Axes of the slice: x: 2, y: 2, z: 4, core: 2. Of those that a mesh axis runs over, the one named last changes fastest.
Arguments:
- tokens: bfloat16 [256, 16, 2048], P('tp', ('rep', 'fs')), may hold values from -6 to 6
- mix_gain: float32 [2048], replicated, may hold values from 0.1 to 1.9
- value_weight: bfloat16 [2048, 1024], P('fs', 'tp'), may hold values from -0.125 to 0.125
- gate_weight: bfloat16 [2048, 1024], P('fs', 'tp'), may hold values from -0.125 to 0.125
- conv_taps: float32 [31, 1024], P(None, 'tp'), may hold values from -1 to 1
- head_gain: float32 [1024], P('tp'), may hold values from 0.1 to 1.9
- out_weight: bfloat16 [1024, 2048], P('tp', 'fs'), may hold values from -0.1875 to 0.1875
- ffn_gain: float32 [2048], replicated, may hold values from 0.1 to 1.9
- ffn_gate_weight: bfloat16 [2048, 3072], P('fs', 'tp'), may hold values from -0.125 to 0.125
- ffn_up_weight: bfloat16 [2048, 3072], P('fs', 'tp'), may hold values from -0.125 to 0.125
- down_weight: bfloat16 [3072, 2048], P('tp', 'fs'), may hold values from -0.109375 to 0.109375
Outputs:
- layer_out: bfloat16 [256, 16, 2048], P('tp', ('rep', 'fs'))
All inputs are finite; a program needn't handle non-finite values.
Results may differ from a plain program's by a relative error of at most 0.012.
Values may be sent and summed in bfloat16 or wider, within the bound.
A program may use at most 128 MiB of HBM per device.

v0:
```python
import functools

import jax
import jax.numpy as jnp
from jax import lax
from jax.experimental import pallas as pl
from jax.experimental.pallas import tpu as pltpu
from jax.sharding import PartitionSpec as P

HEAD_DIM = 128
MESH = pl.DeviceIdType.MESH

norm_eps = 1e-06
group_eps = 1e-05
f32 = jnp.float32
bf16 = jnp.bfloat16


def rms_scale(matrix, scales):
    return matrix * lax.rsqrt(jnp.mean(matrix * matrix, axis=-1, keepdims=True) + norm_eps) * scales


class Moves:
    def __init__(self, n_rep, n_fs, sources, wholes, axes, sems):
        self.rep, self.fs, self.tp = lax.axis_index("rep"), lax.axis_index("fs"), lax.axis_index("tp")
        rep, fs, tp = self.rep, self.fs, self.tp
        self.ring = n_fs // 2
        self.pair, self.place = fs % 2, fs // 2
        flip = fs + 1 - 2 * self.pair
        self.to_tp = (rep, fs, 1 - tp)
        self.peers = (None, (rep, flip, tp), (1 - rep, fs, tp), (1 - rep, flip, tp))
        self.after = (rep, (fs + 2) % n_fs, tp)
        self.before = (rep, (fs + n_fs - 2) % n_fs, tp)
        self.quarter = rep * 2 + self.pair
        self.other = rep * 2 + 1 - self.pair
        self.sources, self.wholes, self.axes = sources, wholes, axes
        self.ring_send, self.ring_recv, self.pair_send, self.pair_recv = sems

    def barrier(self):
        sem = pltpu.get_barrier_semaphore()
        others = self.peers[1:] + (self.to_tp, self.after, self.before)
        for device in others:
            pl.semaphore_signal(sem, inc=1, device_id=device, device_id_type=MESH)
        pl.semaphore_wait(sem, len(others))

    def part(self, w, quarter):
        size = self.sources[w].shape[self.axes[w]] // 4
        at = pl.ds(pl.multiple_of(quarter * size, size), size)
        return (slice(None), at) if self.axes[w] == 1 else (at, slice(None))

    def slot(self, w, owner):
        if self.axes[w] == 0:
            return (owner,)
        size = self.sources[w].shape[0]
        return (pl.ds(pl.multiple_of(owner * size, size), size), slice(None))

    def pair_copy(self, w):
        return pltpu.make_async_remote_copy(
            src_ref=self.sources[w].at[self.part(w, self.other)],
            dst_ref=self.wholes[w].at[self.slot(w, self.fs)],
            send_sem=self.pair_send.at[w],
            recv_sem=self.pair_recv.at[w],
            device_id=self.peers[1],
            device_id_type=MESH,
        )

    def ring_copy(self, w, p, s):
        parity = self.pair if p == 0 else 1 - self.pair
        owner = ((self.place + self.ring + 1 - s) % self.ring) * 2 + parity
        there = self.wholes[w].at[self.slot(w, owner)]
        here = self.sources[w].at[self.part(w, self.quarter)] if s == 1 and p == 0 else there
        return pltpu.make_async_remote_copy(
            src_ref=here,
            dst_ref=there,
            send_sem=self.ring_send.at[w, p, s - 1],
            recv_sem=self.ring_recv.at[w, p, s - 1],
            device_id=self.after,
            device_id_type=MESH,
        )

    def push(self, w, p, s):
        if s > 1:
            self.ring_copy(w, p, s - 1).wait_recv()
        elif p == 1:
            self.pair_copy(w).wait_recv()
        self.ring_copy(w, p, s).start()

    def arrived(self, w):
        for p in (0, 1):
            self.ring_copy(w, p, self.ring - 1).wait_recv()

    def sent(self):
        for w in range(len(self.sources)):
            self.pair_copy(w).wait_send()
            for p in (0, 1):
                for s in range(1, self.ring):
                    self.ring_copy(w, p, s).wait_send()

    def row_copy(self, src, dst, k, sems):
        return pltpu.make_async_remote_copy(
            src_ref=src,
            dst_ref=dst,
            send_sem=sems[0].at[k],
            recv_sem=sems[1].at[k],
            device_id=self.peers[k] if 0 < k < 4 else self.to_tp,
            device_id_type=MESH,
        )


def ring_scratch(count, n_fs):
    ring = n_fs // 2
    return [pltpu.SemaphoreType.DMA((count, 2, ring - 1))] * 2 + [pltpu.SemaphoreType.DMA((count,))] * 2


def whole_shapes(weights, axes, n_fs):
    shapes = []
    for weight, axis in zip(weights, axes):
        shape = list(weight.shape)
        shape[axis] //= 4
        shapes.append((shape[0] * n_fs, shape[1]) if axis == 1 else (n_fs, *shape))
    return shapes


def first_kernel(
    n_rep, n_fs, own, value, gate, out, rows, value_q, gate_q, out_q,
    ring_send, ring_recv, pair_send, pair_recv, row_send, row_recv, local_sem,
):
    sems = (ring_send, ring_recv, pair_send, pair_recv)
    m = Moves(n_rep, n_fs, (value, gate, out), (value_q, gate_q, out_q), (1, 1, 0), sems)
    row_sems = (row_send, row_recv)
    local = [pltpu.make_async_copy(own, rows.at[0], local_sem.at[3])]
    for w in range(3):
        local.append(
            pltpu.make_async_copy(
                m.sources[w].at[m.part(w, m.quarter)],
                m.wholes[w].at[m.slot(w, m.fs)],
                local_sem.at[w],
            )
        )
    for copy in local:
        copy.start()
    m.barrier()
    for w in range(3):
        m.pair_copy(w).start()
        m.push(w, 0, 1)
    near = {k: m.row_copy(own, rows.at[k], k, row_sems) for k in (1, 2, 3)}
    far = {
        k: m.row_copy(own if k == 0 else rows.at[k], rows.at[4 + k], 4 + k, row_sems)
        for k in (0, 1, 2, 3)
    }
    near[3].start()
    near[1].start()
    near[2].start()
    far[0].start()
    for w in range(3):
        m.push(w, 1, 1)
    for s in range(2, m.ring):
        for p in (0, 1):
            for w in range(3):
                m.push(w, p, s)
    for k in (1, 2, 3):
        near[k].wait_recv()
        far[k].start()
    for w in range(3):
        m.arrived(w)
    for k in range(4):
        far[k].wait_recv()
    for copy in local:
        copy.wait()
    for copy in list(near.values()) + list(far.values()):
        copy.wait_send()
    m.sent()


def second_kernel(
    n_rep, n_fs, tokens, act_near, act_far, out_q, ffn_gain, gate, up, down, result,
    gate_q, up_q, down_q, rows, hidden, middle, total, tp_out, tp_in, x_out, x_in,
    ring_send, ring_recv, pair_send, pair_recv, row_send, row_recv, sum_send, sum_recv,
):
    sems = (ring_send, ring_recv, pair_send, pair_recv)
    m = Moves(n_rep, n_fs, (gate, up, down), (gate_q, up_q, down_q), (1, 1, 0), sems)
    row_sems = (row_send, row_recv)
    length, width = tokens.shape
    tile = 512
    high = 32
    m.barrier()
    for w in range(3):
        m.pair_copy(w).start()
    for w in range(2):
        m.push(w, 0, 1)

    def columns(weight, c):
        slots = tile // weight.shape[2]
        return jnp.concatenate([weight[c * slots + i] for i in range(slots)], axis=1)

    def far_sums(phase, far, weight):
        for k in (3, 1, 2, 0):

            def column(c, _):
                at = pl.ds(pl.multiple_of(c * tile, tile), tile)
                tp_out[phase, k, :, at] = jnp.dot(
                    far(k), columns(weight, c), preferred_element_type=f32
                ).astype(bf16)
                return _

            lax.fori_loop(0, width // tile, column, 0)
            tp_copy(phase, k).start()

    def tp_copy(phase, k):
        return m.row_copy(
            tp_out.at[phase, k], tp_in.at[phase, k], 4 + k, (sum_send.at[phase], sum_recv.at[phase])
        )

    def x_copy(phase, k):
        return m.row_copy(
            x_out.at[phase, k - 1], x_in.at[phase, k - 1], k, (sum_send.at[phase], sum_recv.at[phase])
        )

    def near_sums(phase, near, weight):
        for k in (3, 1, 2, 0):
            tp_copy(phase, k).wait_recv()

            def column(c, _):
                at = pl.ds(pl.multiple_of(c * tile, tile), tile)
                part = jnp.dot(near(k), columns(weight, c), preferred_element_type=f32)
                part = part + tp_in[phase, k, :, at].astype(f32)
                if k == 0:
                    total[:, at] = part
                else:
                    x_out[phase, k - 1, :, at] = part.astype(bf16)
                return _

            lax.fori_loop(0, width // tile, column, 0)
            if k:
                x_copy(phase, k).start()

    def all_sums(phase, at):
        part = total[at, :]
        for k in (1, 2, 3):
            part = part + x_in[phase, k - 1, at, :].astype(f32)
        return part

    far_sums(0, lambda k: act_far[k], out_q)
    for w in range(2):
        m.push(w, 1, 1)
    near_sums(0, lambda k: act_near[k], out_q)
    for w in range(3):
        m.wholes[w][m.slot(w, m.fs)] = m.sources[w][m.part(w, m.quarter)]
    for w in range(2):
        m.push(w, 0, 2)
    for w in range(2):
        m.push(w, 1, 2)
    for k in (1, 2, 3):
        x_copy(0, k).wait_recv()

    def norm_rows(i, _):
        at = pl.ds(pl.multiple_of(i * high, high), high)
        mid = (tokens[at, :].astype(f32) + all_sums(0, at)).astype(bf16)
        middle[at, :] = mid
        rows[0, at, :] = rms_scale(mid.astype(f32), ffn_gain[...]).astype(bf16)
        return _

    lax.fori_loop(0, length // high, norm_rows, 0)
    near = {k: m.row_copy(rows.at[0], rows.at[k], k, row_sems) for k in (1, 2, 3)}
    far = {k: m.row_copy(rows.at[k], rows.at[4 + k], 4 + k, row_sems) for k in (0, 1, 2, 3)}
    near[3].start()
    near[1].start()
    near[2].start()
    far[0].start()
    for s in range(3, m.ring):
        for p in (0, 1):
            for w in range(2):
                m.push(w, p, s)
    for p in (0, 1):
        m.push(2, p, 1)
    for k in (1, 2, 3):
        near[k].wait_recv()
        far[k].start()
    for w in range(2):
        m.arrived(w)
    m.push(2, 0, 2)
    for k in range(4):
        far[k].wait_recv()

    def feed(i, _):
        at = pl.ds(2 * i, 2)
        block = rows[at].reshape(2 * length, width)
        gate_part = jnp.dot(block, gate_q[...], preferred_element_type=f32)
        up_part = jnp.dot(block, up_q[...], preferred_element_type=f32)
        hidden[at] = (jax.nn.silu(gate_part) * up_part).astype(bf16).reshape(2, length, -1)
        return _

    lax.fori_loop(0, 4, feed, 0)
    m.push(2, 1, 2)
    for s in range(3, m.ring):
        for p in (0, 1):
            m.push(2, p, s)
    m.arrived(2)
    far_sums(1, lambda k: hidden[4 + k], down_q)
    near_sums(1, lambda k: hidden[k], down_q)
    for k in (1, 2, 3):
        x_copy(1, k).wait_recv()

    def finish(i, _):
        at = pl.ds(pl.multiple_of(i * high, high), high)
        result[at, :] = (middle[at, :].astype(f32) + all_sums(1, at)).astype(bf16)
        return _

    lax.fori_loop(0, length // high, finish, 0)
    for copy in list(near.values()) + list(far.values()):
        copy.wait_send()
    for phase in (0, 1):
        for k in range(4):
            tp_copy(phase, k).wait_send()
        for k in (1, 2, 3):
            x_copy(phase, k).wait_send()
    m.sent()


def body(
    tokens,
    mix_gain,
    value_weight,
    gate_weight,
    conv_taps,
    head_gain,
    out_weight,
    ffn_gain,
    ffn_gate_weight,
    ffn_up_weight,
    down_weight,
):
    n_rep, n_fs, n_tp = lax.axis_size("rep"), lax.axis_size("fs"), lax.axis_size("tp")
    rep, fs, tp = lax.axis_index("rep"), lax.axis_index("fs"), lax.axis_index("tp")
    pair = fs % 2
    local_len, seq_count, width = tokens.shape
    assert n_rep == 2 and n_tp == 2 and n_fs % 2 == 0 and seq_count == 1
    mine_q = rep * 2 + pair
    vmem, anywhere = pl.BlockSpec(memory_space=pltpu.VMEM), pl.BlockSpec(memory_space=pl.ANY)
    sem = pltpu.SemaphoreType.DMA

    rows = tokens.reshape(local_len, width)
    own = rms_scale(rows.astype(f32), mix_gain).astype(bf16)
    module_weights = (value_weight, gate_weight, out_weight)
    shapes = whole_shapes(module_weights, (1, 1, 0), n_fs)
    normed, value_q, gate_q, out_q = pl.pallas_call(
        functools.partial(first_kernel, n_rep, n_fs),
        out_shape=[jax.ShapeDtypeStruct(s, bf16) for s in [(8, local_len, width)] + shapes],
        in_specs=[vmem] * 4,
        out_specs=[anywhere] * 4,
        scratch_shapes=ring_scratch(3, n_fs) + [sem((8,)), sem((8,)), sem((4,))],
        compiler_params=pltpu.CompilerParams(collective_id=0, has_side_effects=True),
    )(own, *module_weights)
    normed = normed.reshape(8 * local_len, width)

    value_rows = jnp.dot(normed, value_q, preferred_element_type=f32)
    gate_rows = jnp.dot(normed, gate_q, preferred_element_type=f32)
    glu = (value_rows * jax.nn.sigmoid(gate_rows)).astype(bf16)
    channels = glu.shape[1]
    glu = glu.reshape(2, 4, local_len, channels)
    first = jnp.where(tp == 0, glu[0], glu[1])
    second = jnp.where(tp == 0, glu[1], glu[0])
    sequence = jnp.concatenate([first, second], axis=1)
    taps = lax.dynamic_slice_in_dim(conv_taps, mine_q * channels, channels, 1)
    gains = lax.dynamic_slice_in_dim(head_gain, mine_q * channels, channels, 0)
    kernel = taps.shape[0]
    conved = lax.conv_general_dilated(
        sequence.astype(f32),
        taps[:, None, :],
        (1,),
        [(kernel // 2, kernel // 2)],
        dimension_numbers=("NWC", "WIO", "NWC"),
        feature_group_count=channels,
        precision=lax.Precision.HIGHEST,
    )
    grouped = conved.reshape(4, 2 * local_len, channels // HEAD_DIM, HEAD_DIM)
    head_mean = jnp.mean(grouped, axis=-1, keepdims=True)
    head_var = jnp.mean(jnp.square(grouped - head_mean), axis=-1, keepdims=True)
    scaled = (grouped - head_mean) * lax.rsqrt(head_var + group_eps) * gains.reshape(-1, HEAD_DIM)
    activated = jax.nn.silu(scaled).astype(bf16).reshape(4, 2 * local_len, channels)
    near = lax.dynamic_slice_in_dim(activated, tp * local_len, local_len, 1)
    far = lax.dynamic_slice_in_dim(activated, (1 - tp) * local_len, local_len, 1)
    ffn_weights = (ffn_gate_weight, ffn_up_weight, down_weight)
    shapes = whole_shapes(ffn_weights, (1, 1, 0), n_fs)
    units = shapes[0][1]
    layer_rows = pl.pallas_call(
        functools.partial(second_kernel, n_rep, n_fs),
        out_shape=jax.ShapeDtypeStruct((local_len, width), bf16),
        in_specs=[vmem] * 8,
        out_specs=vmem,
        scratch_shapes=[pltpu.VMEM(s, bf16) for s in shapes]
        + [
            pltpu.VMEM((8, local_len, width), bf16),
            pltpu.VMEM((8, local_len, units), bf16),
            pltpu.VMEM((local_len, width), bf16),
            pltpu.VMEM((local_len, width), f32),
            pltpu.VMEM((2, 4, local_len, width), bf16),
            pltpu.VMEM((2, 4, local_len, width), bf16),
            pltpu.VMEM((2, 3, local_len, width), bf16),
            pltpu.VMEM((2, 3, local_len, width), bf16),
        ]
        + ring_scratch(3, n_fs)
        + [sem((8,)), sem((8,)), sem((2, 8)), sem((2, 8))],
        compiler_params=pltpu.CompilerParams(
            collective_id=1, has_side_effects=True, vmem_limit_bytes=56 * 1024 * 1024
        ),
    )(rows, near, far, out_q, ffn_gain.reshape(1, width), *ffn_weights)
    return layer_rows.reshape(local_len, seq_count, width)


def solution(mesh):
    placed = (
        P("tp", ("rep", "fs"), None),
        P(),
        P("fs", "tp"),
        P("fs", "tp"),
        P(None, "tp"),
        P("tp"),
        P("tp", "fs"),
        P(),
        P("fs", "tp"),
        P("fs", "tp"),
        P("tp", "fs"),
    )
    return jax.shard_map(
        body, mesh=mesh, in_specs=placed, out_specs=P("tp", ("rep", "fs"), None), check_vma=False
    )
```

profile of v0, /device:TPU:0, one launch (start us, length us, event | category | flops | bytes accessed | tf_op | source)
XLA Modules:
  0.0 178.8 jit_solution(12644626729394109241)
XLA Ops:
  0.0 0.0 copy-start
  0.0 0.8 copy-done
  0.9 1.2 fusion.4
  2.1 2.0 %fusion.6.own = bf16[128,2048]{1,0:T(8,128)(2,1)} fusion(f32[2048]{0:T(1024)} %param.12, f32[128]{0:T(128)S(1)} %add_rsqrt_fusion.1, bf16[128,1,2048]{2,0,1:T(8,128)(2,1)} %param.11), kind=kLoop, calls=%fused_computation.10 | loop fusion | flops 1048576 | bytes 1057280 | tf_op jit(solution)/shard_map/convert_element_type | solution.py:343
  4.1 45.7 %shard_map.109 = (bf16[8,128,2048]{2,1,0:T(8,128)(2,1)}, bf16[2048,128]{1,0:T(8,128)(2,1)}, bf16[2048,128]{1,0:T(8,128)(2,1)}, bf16[8,128,256]{2,1,0:T(8,128)(2,1)}) custom-call(bf16[128,2048]{1,0:T(8,128)(2,1)} %fusion.6.own, bf16[256,512]{1,0:T(8,128)(2,1)} %value.1, bf16[256,512]{1,0:T(8,128)(2,1)} %gate.2, bf16[512,256]{1,0:T(8,128)(2,1)} %out.1), custom_call_target="tpu_custom_call" | custom-call | tf_op jit(solution)/shard_map/pallas_call | solution.py:346
  49.8 0.0 copy-start.1
  49.8 0.0 copy-start.2
  49.8 3.7 %fusion.2 = f32[1024,128]{1,0:T(8,128)S(1)} fusion(bf16[1024,2048]{1,0:T(8,128)(2,1)} %bitcast.13, bf16[2048,128]{1,0:T(8,128)(2,1)} %get-tuple-element.11), kind=kOutput, calls=%fused_computation.6 | convolution fusion | flops 537264128 | bytes 5242880 | tf_op jit(solution)/shard_map/dot_general | solution.py:357
  53.6 0.0 copy-done.1
  53.6 0.0 copy-done.2
  53.6 1.2 fusion.3
  54.9 0.1 copy.26
  55.0 0.1 copy.27
  55.1 3.2 %fusion.12 = (f32[4,256]{0,1:T(8,128)S(1)}, f32[4,256,128]{2,0,1:T(4,128)S(1)}) fusion(f32[31,1,128]{2,1,0:T(1,128)S(1)} %broadcast_in_dim.2, bf16[4,128,128]{2,0,1:T(4,128)(2,1)S(1)} %copy.27, bf16[4,128,128]{2,0,1:T(4,128)(2,1)S(1)} %copy.26), kind=kOutput, calls=%fused_computation.27 | convolution fusion | flops 47938560 | bytes 806400 | tf_op jit(solution)/shard_map/conv_general_dilated | solution.py:367
  58.3 0.1 copy.28
  58.3 0.4 multiply_reduce_fusion
  58.7 0.8 dynamic_slice.13
  59.5 0.4 multiply_convert_fusion
  59.9 0.7 constant_dynamic-slice_fusion
  60.6 116.3 %shard_map.110 = bf16[128,2048]{1,0:T(8,128)(2,1)} custom-call(bf16[128,2048]{1,0:T(8,128)(2,1)} %bitcast.15, bf16[4,128,128]{2,1,0:T(8,128)(2,1)} %get-tuple-element.14.act_near, bf16[4,128,128]{2,1,0:T(8,128)(2,1)} %get-tuple-element.13.act_far, bf16[8,128,256]{2,1,0:T(8,128)(2,1)} %get-tuple-element.12.out_q, f32[1,2048]{1,0:T(1,128)} %bitcast.19, ...), custom_call_target="tpu_custom_call" | custom-call | tf_op jit(solution)/shard_map/pallas_call | solution.py:386
  176.9 1.9 %copy.36 = bf16[128,1,2048]{2,0,1:T(8,128)(2,1)} copy(bf16[128,1,2048]{2,0,1:T(8,128)(2,1)} %bitcast.16) | data formatting | bytes 1048576
  (6 shorter events, 0.1 us)
Async XLA Ops:
  0.0 0.8 copy-start
  49.8 3.7 %copy-start.1 = (bf16[8,128,2048]{2,1,0:T(8,128)(2,1)S(1)}, bf16[8,128,2048]{2,1,0:T(8,128)(2,1)}, u32[]{:S(2)}) copy-start(bf16[8,128,2048]{2,1,0:T(8,128)(2,1)} %get-tuple-element.9) | copy-start | bytes 12582916
  49.8 3.7 %copy-start.2 = (bf16[2048,128]{1,0:T(8,128)(2,1)S(1)}, bf16[2048,128]{1,0:T(8,128)(2,1)}, u32[]{:S(2)}) copy-start(bf16[2048,128]{1,0:T(8,128)(2,1)} %get-tuple-element.10) | copy-start | bytes 1572868
where the time goes:
time: 179 us
  Pallas kernels  162 us (91%)
  matrix products  8.13 us (5%)
  local copies, waits for them, and re-layouts  4.51 us (3%)
  other arithmetic  4.07 us (2%)
    pallas_call x1, Pallas kernels, body(): pl.pallas_call(functools.partial(second_kernel, n_rep, n_fs), out_shape=j...  116 us
    pallas_call x1, Pallas kernels, body(): pl.pallas_call(functools.partial(first_kernel, n_rep, n_fs), out_shape=[j...  45.7 us
    dot_general x1, matrix products, body(): gate_rows = jnp.dot(normed, gate_q, preferred_element_type=f32)  3.71 us

commit v1 on v0

--- a/solution.py
+++ b/solution.py
@@ -96,15 +96,58 @@
                 for s in range(1, self.ring):
                     self.ring_copy(w, p, s).wait_send()
 
-    def row_copy(self, src, dst, k, sems):
+    def copy(self, src, dst, device, sems, i):
         return pltpu.make_async_remote_copy(
             src_ref=src,
             dst_ref=dst,
-            send_sem=sems[0].at[k],
-            recv_sem=sems[1].at[k],
-            device_id=self.peers[k] if 0 < k < 4 else self.to_tp,
+            send_sem=sems[0].at[i],
+            recv_sem=sems[1].at[i],
+            device_id=device,
             device_id_type=MESH,
         )
+
+
+class RowGather:
+    def __init__(self, m, own, rows, sems):
+        half = own.shape[0] // 2
+        low, high = pl.ds(0, half), pl.ds(half, half)
+        _, pair, rep, _ = m.peers
+        moves = (
+            (own.at[low], rows.at[2, low], rep),
+            (own.at[high], rows.at[1, high], pair),
+            (own.at[high], rows.at[2, high], rep),
+            (own.at[low], rows.at[1, low], pair),
+            (rows.at[2, low], rows.at[3, low], pair),
+            (rows.at[1, high], rows.at[3, high], rep),
+            (own, rows.at[4], m.to_tp),
+            (rows.at[2], rows.at[6], m.to_tp),
+            (rows.at[1], rows.at[5], m.to_tp),
+            (rows.at[3, low], rows.at[7, low], m.to_tp),
+            (rows.at[3, high], rows.at[7, high], m.to_tp),
+        )
+        self.copies = [m.copy(*move, sems, i) for i, move in enumerate(moves)]
+
+    def start(self):
+        for i in (0, 1, 2, 3, 6):
+            self.copies[i].start()
+
+    def forward(self):
+        for i in (0, 1):
+            self.copies[i].wait_recv()
+            self.copies[i + 4].start()
+
+    def finish(self):
+        for i in (2, 3, 4, 5):
+            self.copies[i].wait_recv()
+            self.copies[i + 5].start()
+
+    def arrived(self):
+        for i in range(6, 11):
+            self.copies[i].wait_recv()
+
+    def sent(self):
+        for copy in self.copies:
+            copy.wait_send()
 
 
 def ring_scratch(count, n_fs):
@@ -143,32 +186,22 @@
     for w in range(3):
         m.pair_copy(w).start()
         m.push(w, 0, 1)
-    near = {k: m.row_copy(own, rows.at[k], k, row_sems) for k in (1, 2, 3)}
-    far = {
-        k: m.row_copy(own if k == 0 else rows.at[k], rows.at[4 + k], 4 + k, row_sems)
-        for k in (0, 1, 2, 3)
-    }
-    near[3].start()
-    near[1].start()
-    near[2].start()
-    far[0].start()
+    gather = RowGather(m, own, rows, row_sems)
+    gather.start()
     for w in range(3):
         m.push(w, 1, 1)
+    gather.forward()
     for s in range(2, m.ring):
         for p in (0, 1):
             for w in range(3):
                 m.push(w, p, s)
-    for k in (1, 2, 3):
-        near[k].wait_recv()
-        far[k].start()
+    gather.finish()
     for w in range(3):
         m.arrived(w)
-    for k in range(4):
-        far[k].wait_recv()
+    gather.arrived()
     for copy in local:
         copy.wait()
-    for copy in list(near.values()) + list(far.values()):
-        copy.wait_send()
+    gather.sent()
     m.sent()
 
 
@@ -193,65 +226,115 @@
         slots = tile // weight.shape[2]
         return jnp.concatenate([weight[c * slots + i] for i in range(slots)], axis=1)
 
-    def far_sums(phase, far, weight):
-        for k in (3, 1, 2, 0):
-
-            def column(c, _):
-                at = pl.ds(pl.multiple_of(c * tile, tile), tile)
-                tp_out[phase, k, :, at] = jnp.dot(
-                    far(k), columns(weight, c), preferred_element_type=f32
-                ).astype(bf16)
+    def tile_loop(step):
+        def run(c, _):
+            step(columns(out_q, c), pl.ds(pl.multiple_of(c * tile, tile), tile))
+            return _
+
+        lax.fori_loop(0, width // tile, run, 0)
+
+    def phase_columns(phase):
+        if phase == 0:
+            return slice(None)
+        size = 2 * width // n_fs
+        owner = (m.place + m.ring + 1 - phase) % m.ring
+        return pl.ds(pl.multiple_of(owner * size, size), size)
+
+    def for_columns(phase, step):
+        if phase == 0:
+            tile_loop(step)
+        else:
+            owner = ((m.place + m.ring + 1 - phase) % m.ring) * 2
+            weight = jnp.concatenate([down_q[owner], down_q[owner + 1]], axis=1)
+            step(weight, phase_columns(phase))
+
+    def tp_copy(phase, k):
+        b, at = min(phase, 1), phase_columns(phase)
+        phase_sems = (sum_send.at[phase], sum_recv.at[phase])
+        return m.copy(tp_out.at[b, k, :, at], tp_in.at[b, k, :, at], m.to_tp, phase_sems, k)
+
+    def x_copy(phase, k, low):
+        b, columns_at = min(phase, 1), phase_columns(phase)
+        at = pl.ds(0, length // 2) if low else pl.ds(length // 2, length // 2)
+        to_rep = k == 2 or (k == 3 and low)
+        return m.copy(
+            x_out.at[b, k - 1, at, columns_at],
+            x_in.at[b, k - 1, at, columns_at],
+            m.peers[2 if to_rep else 1],
+            (sum_send.at[phase], sum_recv.at[phase]),
+            2 * k + 2 + low,
+        )
+
+    def far_sums(phase, far):
+        b = min(phase, 1)
+        for k in (3, 2, 1, 0):
+
+            def step(weight, at):
+                product = jnp.dot(far(k), weight, preferred_element_type=f32)
+                tp_out[b, k, :, at] = product.astype(bf16)
+
+            for_columns(phase, step)
+            tp_copy(phase, k).start()
+
+    def near_sums(phase, near):
+        b = min(phase, 1)
+        for k in (3, 2, 1, 0):
+            tp_copy(phase, k).wait_recv()
+
+            def step(weight, at):
+                part = jnp.dot(near(k), weight, preferred_element_type=f32)
+                part = part + tp_in[b, k, :, at].astype(f32)
+                if k == 0:
+                    total[b, :, at] = part
+                else:
+                    x_out[b, k - 1, :, at] = part.astype(bf16)
+
+            for_columns(phase, step)
+            if k == 3:
+                x_copy(phase, 3, 1).start()
+                x_copy(phase, 3, 0).start()
+            elif k:
+                x_copy(phase, k, k - 1).start()
+
+    def forward_sums(phase):
+        b, columns_at = min(phase, 1), phase_columns(phase)
+        for k, low in ((1, 1), (2, 0)):
+            x_copy(phase, 3, low).wait_recv()
+            first = 0 if low else length // 2
+
+            def add(i, _):
+                at = pl.ds(pl.multiple_of(first + i * high, high), high)
+                part = x_out[b, k - 1, at, columns_at].astype(f32)
+                part = part + x_in[b, 2, at, columns_at].astype(f32)
+                x_out[b, k - 1, at, columns_at] = part.astype(bf16)
                 return _
 
-            lax.fori_loop(0, width // tile, column, 0)
-            tp_copy(phase, k).start()
-
-    def tp_copy(phase, k):
-        return m.row_copy(
-            tp_out.at[phase, k], tp_in.at[phase, k], 4 + k, (sum_send.at[phase], sum_recv.at[phase])
-        )
-
-    def x_copy(phase, k):
-        return m.row_copy(
-            x_out.at[phase, k - 1], x_in.at[phase, k - 1], k, (sum_send.at[phase], sum_recv.at[phase])
-        )
-
-    def near_sums(phase, near, weight):
-        for k in (3, 1, 2, 0):
-            tp_copy(phase, k).wait_recv()
-
-            def column(c, _):
-                at = pl.ds(pl.multiple_of(c * tile, tile), tile)
-                part = jnp.dot(near(k), columns(weight, c), preferred_element_type=f32)
-                part = part + tp_in[phase, k, :, at].astype(f32)
-                if k == 0:
-                    total[:, at] = part
-                else:
-                    x_out[phase, k - 1, :, at] = part.astype(bf16)
-                return _
-
-            lax.fori_loop(0, width // tile, column, 0)
-            if k:
-                x_copy(phase, k).start()
-
-    def all_sums(phase, at):
-        part = total[at, :]
-        for k in (1, 2, 3):
-            part = part + x_in[phase, k - 1, at, :].astype(f32)
+            lax.fori_loop(0, length // (2 * high), add, 0)
+            x_copy(phase, k, low).start()
+
+    def sums_arrived(phase):
+        for k in (1, 2):
+            for low in (0, 1):
+                x_copy(phase, k, low).wait_recv()
+
+    def all_sums(b, at):
+        part = total[b, at, :]
+        for k in (1, 2):
+            part = part + x_in[b, k - 1, at, :].astype(f32)
         return part
 
-    far_sums(0, lambda k: act_far[k], out_q)
+    far_sums(0, lambda k: act_far[k])
     for w in range(2):
         m.push(w, 1, 1)
-    near_sums(0, lambda k: act_near[k], out_q)
+    near_sums(0, lambda k: act_near[k])
     for w in range(3):
         m.wholes[w][m.slot(w, m.fs)] = m.sources[w][m.part(w, m.quarter)]
     for w in range(2):
         m.push(w, 0, 2)
+    forward_sums(0)
     for w in range(2):
         m.push(w, 1, 2)
-    for k in (1, 2, 3):
-        x_copy(0, k).wait_recv()
+    sums_arrived(0)
 
     def norm_rows(i, _):
         at = pl.ds(pl.multiple_of(i * high, high), high)
@@ -261,26 +344,23 @@
         return _
 
     lax.fori_loop(0, length // high, norm_rows, 0)
-    near = {k: m.row_copy(rows.at[0], rows.at[k], k, row_sems) for k in (1, 2, 3)}
-    far = {k: m.row_copy(rows.at[k], rows.at[4 + k], 4 + k, row_sems) for k in (0, 1, 2, 3)}
-    near[3].start()
-    near[1].start()
-    near[2].start()
-    far[0].start()
+    gather = RowGather(m, rows.at[0], rows, row_sems)
+    gather.start()
     for s in range(3, m.ring):
         for p in (0, 1):
             for w in range(2):
                 m.push(w, p, s)
+            if s == 3 and p == 0:
+                gather.forward()
+    if m.ring < 4:
+        gather.forward()
     for p in (0, 1):
         m.push(2, p, 1)
-    for k in (1, 2, 3):
-        near[k].wait_recv()
-        far[k].start()
+    gather.finish()
     for w in range(2):
         m.arrived(w)
     m.push(2, 0, 2)
-    for k in range(4):
-        far[k].wait_recv()
+    gather.arrived()
 
     def feed(i, _):
         at = pl.ds(2 * i, 2)
@@ -292,14 +372,19 @@
 
     lax.fori_loop(0, 4, feed, 0)
     m.push(2, 1, 2)
-    for s in range(3, m.ring):
-        for p in (0, 1):
-            m.push(2, p, s)
-    m.arrived(2)
-    far_sums(1, lambda k: hidden[4 + k], down_q)
-    near_sums(1, lambda k: hidden[k], down_q)
-    for k in (1, 2, 3):
-        x_copy(1, k).wait_recv()
+    for t in range(m.ring):
+        if t == m.ring - 1:
+            m.arrived(2)
+        elif t > 1:
+            for p in (0, 1):
+                m.push(2, p, t + 1)
+        far_sums(1 + t, lambda k: hidden[4 + k])
+        near_sums(1 + t, lambda k: hidden[k])
+        if t:
+            forward_sums(t)
+    forward_sums(m.ring)
+    for t in range(m.ring):
+        sums_arrived(1 + t)
 
     def finish(i, _):
         at = pl.ds(pl.multiple_of(i * high, high), high)
@@ -307,13 +392,13 @@
         return _
 
     lax.fori_loop(0, length // high, finish, 0)
-    for copy in list(near.values()) + list(far.values()):
-        copy.wait_send()
-    for phase in (0, 1):
+    gather.sent()
+    for phase in range(1 + m.ring):
         for k in range(4):
             tp_copy(phase, k).wait_send()
         for k in (1, 2, 3):
-            x_copy(phase, k).wait_send()
+            for low in (0, 1):
+                x_copy(phase, k, low).wait_send()
     m.sent()
 
 
@@ -348,7 +433,7 @@
         out_shape=[jax.ShapeDtypeStruct(s, bf16) for s in [(8, local_len, width)] + shapes],
         in_specs=[vmem] * 4,
         out_specs=[anywhere] * 4,
-        scratch_shapes=ring_scratch(3, n_fs) + [sem((8,)), sem((8,)), sem((4,))],
+        scratch_shapes=ring_scratch(3, n_fs) + [sem((11,)), sem((11,)), sem((4,))],
         compiler_params=pltpu.CompilerParams(collective_id=0, has_side_effects=True),
     )(own, *module_weights)
     normed = normed.reshape(8 * local_len, width)
@@ -393,14 +478,14 @@
             pltpu.VMEM((8, local_len, width), bf16),
             pltpu.VMEM((8, local_len, units), bf16),
             pltpu.VMEM((local_len, width), bf16),
-            pltpu.VMEM((local_len, width), f32),
+            pltpu.VMEM((2, local_len, width), f32),
             pltpu.VMEM((2, 4, local_len, width), bf16),
             pltpu.VMEM((2, 4, local_len, width), bf16),
             pltpu.VMEM((2, 3, local_len, width), bf16),
             pltpu.VMEM((2, 3, local_len, width), bf16),
         ]
         + ring_scratch(3, n_fs)
-        + [sem((8,)), sem((8,)), sem((2, 8)), sem((2, 8))],
+        + [sem((11,)), sem((11,)), sem((1 + n_fs // 2, 10)), sem((1 + n_fs // 2, 10))],
         compiler_params=pltpu.CompilerParams(
             collective_id=1, has_side_effects=True, vmem_limit_bytes=56 * 1024 * 1024
         ),

time: 179 us -> 148 us (0.83)
  Pallas kernels: 162 us -> 130 us
    pallas_call x1, Pallas kernels: 116 us -> 93 us  [body(): pl.pallas_call(functools.partial(second_kernel, n_rep, n_fs), out_shape=j...]
    pallas_call x1, Pallas kernels: 45.7 us -> 37.4 us  [body(): pl.pallas_call(functools.partial(first_kernel, n_rep, n_fs), out_shape=[j...]
where the time goes in v1:
time: 148 us; the launch traced here: 147 us
  Pallas kernels  130 us (88%)
  matrix products  8.12 us (5%)
  local copies, waits for them, and re-layouts  4.51 us (3%)
  other arithmetic  4.07 us (3%)
    pallas_call x1, Pallas kernels, body(): pl.pallas_call(functools.partial(second_kernel, n_rep, n_fs), out_shape=j...  93 us
    pallas_call x1, Pallas kernels, body(): pl.pallas_call(functools.partial(first_kernel, n_rep, n_fs), out_shape=[j...  37.4 us
    dot_general x1, matrix products, body(): gate_rows = jnp.dot(normed, gate_q, preferred_element_type=f32)  3.71 us
    conv_general_dilated x1, matrix products, body(): lax.conv_general_dilated(sequence.astype(f32), taps[:, None, :], (1,), [(...  3.17 us

profile of v1, /device:TPU:0, one launch (start us, length us, event | category | flops | bytes accessed | tf_op | source)
XLA Modules:
  0.0 147.2 jit_solution(884289334190769585)
XLA Ops:
  0.0 0.0 copy-start
  0.0 0.8 copy-done
  0.9 1.2 fusion.4
  2.1 2.0 %fusion.6.own = bf16[128,2048]{1,0:T(8,128)(2,1)} fusion(f32[2048]{0:T(1024)} %param.12, f32[128]{0:T(128)S(1)} %add_rsqrt_fusion.1, bf16[128,1,2048]{2,0,1:T(8,128)(2,1)} %param.11), kind=kLoop, calls=%fused_computation.10 | loop fusion | flops 1048576 | bytes 1057280 | tf_op jit(solution)/shard_map/convert_element_type | solution.py:428
  4.1 37.4 %shard_map.109 = (bf16[8,128,2048]{2,1,0:T(8,128)(2,1)}, bf16[2048,128]{1,0:T(8,128)(2,1)}, bf16[2048,128]{1,0:T(8,128)(2,1)}, bf16[8,128,256]{2,1,0:T(8,128)(2,1)}) custom-call(bf16[128,2048]{1,0:T(8,128)(2,1)} %fusion.6.own, bf16[256,512]{1,0:T(8,128)(2,1)} %value.1, bf16[256,512]{1,0:T(8,128)(2,1)} %gate.2, bf16[512,256]{1,0:T(8,128)(2,1)} %out.1), custom_call_target="tpu_custom_call" | custom-call | tf_op jit(solution)/shard_map/pallas_call | solution.py:431
  41.5 0.0 copy-start.1
  41.5 0.0 copy-start.2
  41.5 3.7 %fusion.2 = f32[1024,128]{1,0:T(8,128)S(1)} fusion(bf16[1024,2048]{1,0:T(8,128)(2,1)} %bitcast.13, bf16[2048,128]{1,0:T(8,128)(2,1)} %get-tuple-element.11), kind=kOutput, calls=%fused_computation.6 | convolution fusion | flops 537264128 | bytes 5242880 | tf_op jit(solution)/shard_map/dot_general | solution.py:442
  45.2 0.0 copy-done.1
  45.3 0.0 copy-done.2
  45.3 1.2 fusion.3
  46.6 0.1 copy.26
  46.7 0.1 copy.27
  46.8 3.2 %fusion.12 = (f32[4,256]{0,1:T(8,128)S(1)}, f32[4,256,128]{2,0,1:T(4,128)S(1)}) fusion(f32[31,1,128]{2,1,0:T(1,128)S(1)} %broadcast_in_dim.2, bf16[4,128,128]{2,0,1:T(4,128)(2,1)S(1)} %copy.27, bf16[4,128,128]{2,0,1:T(4,128)(2,1)S(1)} %copy.26), kind=kOutput, calls=%fused_computation.27 | convolution fusion | flops 47938560 | bytes 806400 | tf_op jit(solution)/shard_map/conv_general_dilated | solution.py:452
  50.0 0.1 copy.28
  50.0 0.4 multiply_reduce_fusion
  50.4 0.8 dynamic_slice.13
  51.2 0.4 multiply_convert_fusion
  51.6 0.7 constant_dynamic-slice_fusion
  52.3 93.0 %shard_map.110 = bf16[128,2048]{1,0:T(8,128)(2,1)} custom-call(bf16[128,2048]{1,0:T(8,128)(2,1)} %bitcast.15, bf16[4,128,128]{2,1,0:T(8,128)(2,1)} %get-tuple-element.14.act_near, bf16[4,128,128]{2,1,0:T(8,128)(2,1)} %get-tuple-element.13.act_far, bf16[8,128,256]{2,1,0:T(8,128)(2,1)} %get-tuple-element.12.out_q, f32[1,2048]{1,0:T(1,128)} %bitcast.19, ...), custom_call_target="tpu_custom_call" | custom-call | tf_op jit(solution)/shard_map/pallas_call | solution.py:471
  145.3 1.9 %copy.36 = bf16[128,1,2048]{2,0,1:T(8,128)(2,1)} copy(bf16[128,1,2048]{2,0,1:T(8,128)(2,1)} %bitcast.16) | data formatting | bytes 1048576
  (6 shorter events, 0.1 us)
Async XLA Ops:
  0.0 0.8 copy-start
  41.5 3.7 %copy-start.1 = (bf16[8,128,2048]{2,1,0:T(8,128)(2,1)S(1)}, bf16[8,128,2048]{2,1,0:T(8,128)(2,1)}, u32[]{:S(2)}) copy-start(bf16[8,128,2048]{2,1,0:T(8,128)(2,1)} %get-tuple-element.9) | copy-start | bytes 12582916
  41.5 3.7 %copy-start.2 = (bf16[2048,128]{1,0:T(8,128)(2,1)S(1)}, bf16[2048,128]{1,0:T(8,128)(2,1)}, u32[]{:S(2)}) copy-start(bf16[2048,128]{1,0:T(8,128)(2,1)} %get-tuple-element.10) | copy-start | bytes 1572868
